TPU v7x, 32 devices: a whole 2x2x4 slice. The times are simulated.
32 devices in a mesh: rep: 2 (over x), fs: 8 (over z, y), tp: 2 (over core).
Axes of the slice: x: 2, y: 2, z: 4, core: 2. Of those that a mesh axis runs over, the one named last changes fastest.
Arguments:
- inputs: bfloat16 [4096, 2048], P(('rep', 'fs', 'tp')), may hold values from -6 to 6
- cotangent: bfloat16 [4096, 2048], P(('rep', 'fs', 'tp')), may hold values from -6 to 6
- up_weight: bfloat16 [2048, 4096], P('fs', 'tp'), may hold values from -0.125 to 0.125
- down_weight: bfloat16 [4096, 2048], P('tp', 'fs'), may hold values from -0.09375 to 0.09375
Outputs:
- input_grad: bfloat16 [4096, 2048], P(('rep', 'fs', 'tp'))
- up_grad: float32 [2048, 4096], P('fs', 'tp')
- down_grad: float32 [4096, 2048], P('tp', 'fs')
All inputs are finite; a program needn't handle non-finite values.
Results may differ from a plain program's by a relative error of at most 0.013.
Values may be sent and summed in bfloat16 or wider, within the bound.
A program may use at most 128 MiB of HBM per device.

v0:
```python
import math

import jax
import jax.numpy as jnp
from jax import lax
from jax.sharding import PartitionSpec as P


def shards(inputs, cotangent, up_weight, down_weight):
    input_rows, grad_rows = (
        lax.all_gather(inputs, "tp", axis=0, tiled=True),
        lax.all_gather(cotangent, "tp", axis=0, tiled=True),
    )
    up_whole = lax.all_gather(up_weight, "fs", axis=0, tiled=True)
    pre_active = jnp.dot(input_rows, up_whole, preferred_element_type=jnp.float32)
    active = jnp.maximum(pre_active, 0.0)
    activation = (active * active).astype(jnp.bfloat16)
    columns = grad_rows
    activation_grad = lax.dot_general(
        columns,
        lax.all_gather(down_weight, "fs", axis=1, tiled=True),
        (((1,), (1,)), ((), ())),
        preferred_element_type=jnp.float32,
    )
    pre_grad = (2.0 * active * activation_grad).astype(jnp.bfloat16)
    partial_sum = lax.dot_general(
        pre_grad, up_whole, (((1,), (1,)), ((), ())), preferred_element_type=jnp.float32
    )
    input_grad = lax.psum_scatter(
        lax.optimization_barrier(partial_sum.astype(jnp.bfloat16))
        .astype(jnp.float32)
        .astype(jnp.bfloat16),
        "tp",
        scatter_dimension=0,
        tiled=True,
    )
    rep_count = lax.axis_size("rep")
    fs_count = lax.axis_size("fs")
    total_tokens = inputs.shape[0] * rep_count * fs_count * lax.axis_size("tp")
    loss_scale = 1.0 / math.sqrt(total_tokens)
    down_partial = lax.dot_general(
        activation, grad_rows, (((0,), (0,)), ((), ())), preferred_element_type=jnp.float32
    )
    columns = input_rows
    up_piece = lax.psum_scatter(
        lax.dot_general(
            columns, pre_grad, (((0,), (0,)), ((), ())), preferred_element_type=jnp.float32
        ),
        "fs",
        scatter_dimension=0,
        tiled=True,
    )
    down_piece = lax.psum_scatter(down_partial, "fs", scatter_dimension=1, tiled=True)
    up_grad, down_grad = lax.psum((up_piece, down_piece), "rep")
    return (input_grad, up_grad * loss_scale, down_grad * loss_scale)


def solution(mesh):
    placed = (
        P(("rep", "fs", "tp"), None),
        P(("rep", "fs", "tp"), None),
        P("fs", "tp"),
        P("tp", "fs"),
    )
    return jax.shard_map(
        shards,
        mesh=mesh,
        in_specs=placed,
        out_specs=(P(("rep", "fs", "tp"), None), P("fs", "tp"), P("tp", "fs")),
        check_vma=False,
    )
```

profile of v0, /device:TPU:0, one launch (start us, length us, event | category | flops | bytes accessed | tf_op | source)
XLA Modules:
  0.0 978.7 jit_solution(5026646738183738570)
XLA Ops:
  7.2 0.7 all-gather.5.cloned.1.call-update
  7.9 0.7 all-gather.7.cloned.1.call-update
  8.7 0.7 all-gather.9.cloned.1.call-update
  9.4 0.5 all-gather.11.cloned.1.call-update
  10.0 11.3 %all-gather.5.cloned.1.call-done = bf16[256,2048]{1,0:T(8,128)(2,1)} async-done(((bf16[128,2048]{1,0:T(8,128)(2,1)}), bf16[256,2048]{1,0:T(8,128)(2,1)}) %all-gather.5.cloned.1.call-update) | async-done | bytes 1048592 | tf_op jit(solution)/shard_map/all_gather | solution.py:11
  21.3 127.8 %all-gather.7.cloned.1.call-done = bf16[2048,2048]{1,0:T(8,128)(2,1)} async-done(((bf16[256,2048]{1,0:T(8,128)(2,1)}), bf16[2048,2048]{1,0:T(8,128)(2,1)}) %all-gather.7.cloned.1.call-update) | async-done | bytes 8388624 | tf_op jit(solution)/shard_map/all_gather | solution.py:14
  149.1 6.1 convolution_maximum_fusion
  155.2 2.7 all-gather.9.cloned.1.call-done
  157.9 9.4 fusion.1
  167.3 0.0 reduce-scatter.6.cloned.1.call-start
  167.3 118.6 %all-gather.11.cloned.1.call-done = bf16[2048,2048]{1,0:T(8,128)(2,1)} async-done(((bf16[2048,256]{1,0:T(8,128)(2,1)}), bf16[2048,2048]{1,0:T(8,128)(2,1)}) %all-gather.11.cloned.1.call-update) | async-done | bytes 8388624 | tf_op jit(solution)/shard_map/all_gather | solution.py:21
  285.9 6.1 fusion
  292.0 1.0 copy-done.1
  293.0 8.1 convolution_bitcast_fusion
  301.1 0.0 all-reduce.3.cloned.1.call-start
  301.2 266.8 %reduce-scatter.8.cloned.1.call-done = f32[2048,256]{1,0:T(8,128)} async-done(((f32[2048,2048]{1,0:T(8,128)}), f32[2048,256]{1,0:T(8,128)}) %reduce-scatter.8.cloned.1.call-update) | async-done | bytes 2097168 | tf_op jit(solution)/shard_map/reduce_scatter | solution.py:53
  568.0 283.1 %reduce-scatter.6.cloned.1.call-done = f32[256,2048]{0,1:T(8,128)} async-done(((f32[2048,2048]{0,1:T(8,128)}), f32[256,2048]{0,1:T(8,128)}) %reduce-scatter.6.cloned.1.call-update) | async-done | bytes 2097168 | tf_op jit(solution)/shard_map/reduce_scatter | solution.py:45
  851.2 1.2 copy-done.2
  852.3 6.7 convolution_convert_fusion
  859.1 101.6 %all-reduce.3.cloned.1.call-done = (f32[256,2048]{0,1:T(8,128)}, f32[2048,256]{1,0:T(8,128)}) async-done(((f32[256,2048]{0,1:T(8,128)}, f32[2048,256]{1,0:T(8,128)}), (f32[256,2048]{0,1:T(8,128)}, f32[2048,256]{1,0:T(8,128)})) %all-reduce.3.cloned.1.call-update) | async-done | bytes 4194320 | tf_op jit(solution)/shard_map/psum | solution.py:54
  960.6 1.7 broadcast_multiply_fusion.1
  962.4 1.8 copy.7
  964.2 3.0 broadcast_multiply_fusion
  967.2 4.7 reduce-scatter.4.cloned.1.call-done
  (14 shorter events, 0.3 us)
Async XLA Ops:
  7.2 14.1 %all-gather.5.cloned.1.call-start = ((), (), s32[]{:S(2)}) async-start(), calls=%async_computation.3 | async-start | bytes 1572864 | tf_op jit(solution)/shard_map/all_gather | solution.py:11
  7.9 141.2 %all-gather.7.cloned.1.call-start = ((), (), s32[]{:S(2)}) async-start(), calls=%async_computation.4 | async-start | bytes 9437184 | tf_op jit(solution)/shard_map/all_gather | solution.py:14
  8.6 149.3 %all-gather.9.cloned.1.call-start = ((), (), s32[]{:S(2)}) async-start(), calls=%async_computation.5 | async-start | bytes 1572864 | tf_op jit(solution)/shard_map/all_gather | solution.py:12
  9.4 276.6 %all-gather.11.cloned.1.call-start = ((), (), s32[]{:S(2)}) async-start(), calls=%async_computation.6 | async-start | bytes 9437184 | tf_op jit(solution)/shard_map/all_gather | solution.py:21
  10.0 558.1 %reduce-scatter.8.cloned.1.call-start = ((), (), s32[]{:S(2)}) async-start(), calls=%async_computation.9 | async-start | bytes 18874368 | tf_op jit(solution)/shard_map/reduce_scatter | solution.py:53
  167.3 125.7 %copy-start = (bf16[256,2048]{1,0:T(8,128)(2,1)S(1)}, bf16[256,2048]{1,0:T(8,128)(2,1)}, u32[]{:S(2)}) copy-start(bf16[256,2048]{1,0:T(8,128)(2,1)} %all-gather.5.cloned.1.call-done) | copy-start | bytes 3145732
  167.3 683.8 %reduce-scatter.6.cloned.1.call-start = ((), (), s32[]{:S(2)}) async-start(), calls=%async_computation.8 | async-start | bytes 18874368 | tf_op jit(solution)/shard_map/reduce_scatter | solution.py:45
  292.0 1.0 copy-start.1
  301.1 659.5 %all-reduce.3.cloned.1.call-start = ((), (), s32[]{:S(2)}) async-start(), calls=%async_computation.10 | async-start | bytes 8388608 | tf_op jit(solution)/shard_map/psum | solution.py:54
  851.1 1.2 copy-start.2
  851.1 120.8 %reduce-scatter.4.cloned.1.call-start = ((), (), s32[]{:S(2)}) async-start(), calls=%async_computation.7 | async-start | bytes 1572864 | tf_op jit(solution)/shard_map/reduce_scatter | solution.py:29
Sparse Core Ops, SparseCore 0:
  9.5 11.7 all-gather.4
  23.4 125.6 all-gather.6
  150.7 7.1 all-gather.8
  159.8 126.0 all-gather.10
  289.6 278.3 reduce-scatter.7
  571.7 279.3 reduce-scatter.5
  853.6 107.0 all-reduce.2
  963.4 8.3 reduce-scatter.3
where the time goes:
time: 979 us
  waiting for transfers between devices  919 us (94%)
  matrix products  36.3 us (4%)
  between operations  14.2 us (1%)
    reduce_scatter x1, waiting for transfers between devices, shards(): lax.psum_scatter(lax.dot_general(columns, pre_grad, (((0,), (0,)), ((), (...  283 us
    reduce_scatter x1, waiting for transfers between devices, shards(): lax.psum_scatter(down_partial, 'fs', scatter_dimension=1, tiled=True)  267 us
    all_gather x1, waiting for transfers between devices, shards(): up_whole = lax.all_gather(up_weight, 'fs', axis=0, tiled=True)  128 us
    all_gather x1, waiting for transfers between devices, shards(): lax.all_gather(down_weight, 'fs', axis=1, tiled=True)  119 us
    psum x1, waiting for transfers between devices, shards(): up_grad, down_grad = lax.psum((up_piece, down_piece), 'rep')  102 us
  transfers between devices with their start and end apart: 8, of which 8 were waited for; matrix products, arithmetic and copies ran while one was open for 4% of the time, Pallas kernels for 0%

commit v1 on v0

v1 whole, which is shorter than its diff:
```python
import functools
import math

import jax
import jax.numpy as jnp
from jax import lax
from jax.experimental import pallas as pl
from jax.experimental.pallas import tpu as pltpu
from jax.sharding import PartitionSpec as P

MESH = pl.DeviceIdType.MESH
BF16, F32 = jnp.bfloat16, jnp.float32
NT = (((1,), (1,)), ((), ()))


def ring_place(f, n):
    odd = lax.rem(f, 2)
    half = lax.div(f, 2)
    return half * (1 - odd) + (n - 1 - half) * odd


def ring_member(p, n):
    back = lax.div(p, (n + 1) // 2)
    return 2 * p * (1 - back) + (2 * n - 1 - 2 * p) * back


def tile_of(size, most):
    while size % most:
        most //= 2
    return most


def kernel(
    R, n, T,
    x_ref, c_ref, u_ref, d_ref,
    ig_ref, gu_ref, gd_ref,
    xg, cg, xt, ug, dg, pre, agr, pg, at,
    igp, itr, isum, irr, us, ur, ds_, dr_, fu, fd, fur, fdr,
    ag_ss, ag_rs, rs_ss, rs_rs, tr_ss, tr_rs, tt_ss, tt_rs,
    it_ss, it_rs, ir_ss, ir_rs, f_ss, f_rs,
):
    r, f, t = lax.axis_index("rep"), lax.axis_index("fs"), lax.axis_index("tp")
    tok, db = x_ref.shape[1], x_ref.shape[2]
    hb = u_ref.shape[1]
    rows = R * T * tok
    p = ring_place(f, n)

    def member(q):
        return ring_member(lax.rem(p + q + n, n), n)

    def ring_dev(sign):
        return (r, member(sign), t)

    def rep_dev(q):
        return (lax.rem(r + q + R, R), f, t)

    def tp_dev(q):
        return (r, f, lax.rem(t + q + T, T))

    barrier = pltpu.get_barrier_semaphore()
    peers = [ring_dev(1), ring_dev(-1)]
    peers += [rep_dev(q) for q in range(1, R)] + [tp_dev(q) for q in range(1, T)]
    for peer in peers:
        pl.semaphore_signal(barrier, inc=1, device_id=peer, device_id_type=MESH)
    pl.semaphore_wait(barrier, len(peers))

    def remote(src, dst, ssem, rsem, dev):
        return pltpu.make_async_remote_copy(
            src_ref=src, dst_ref=dst, send_sem=ssem, recv_sem=rsem,
            device_id=dev, device_id_type=MESH,
        )

    long, short = n // 2, (n - 1) // 2
    streams = [(0, 1, long), (0, -1, short), (1, 1, short), (1, -1, long)]
    hops = max(long, short)
    own = (u_ref, d_ref)
    held = (ug, dg)

    def slot(sign, s):
        return (n - s if sign > 0 else s) - 1

    def gather_copy(i, s):
        g, sign, _ = streams[i]
        src = own[g] if s == 1 else held[g].at[slot(sign, s - 1)]
        return remote(
            src, held[g].at[slot(sign, s)], ag_ss.at[i, s - 1], ag_rs.at[i, s - 1],
            ring_dev(sign),
        )

    sends = []

    def go(copy):
        copy.start()
        sends.append(copy)
        return copy

    flying = {}
    for i, (g, sign, k) in enumerate(streams):
        if k >= 1:
            flying[i, 1] = go(gather_copy(i, 1))

    tokens = ((x_ref, xg), (c_ref, cg))

    def span(dt, dr):
        return pl.ds((dt * R + dr) * tok, tok)

    rep_copies = {}
    for dr in range(1, R):
        for j, (ref, full) in enumerate(tokens):
            rep_copies[j, dr] = go(remote(
                ref, full.at[:, span(0, dr), :], tr_ss.at[j, dr], tr_rs.at[j, dr], rep_dev(-dr)
            ))
    tp_copies = {}
    for dt in range(1, T):
        for j, (ref, full) in enumerate(tokens):
            tp_copies[j, dt, 0] = go(remote(
                ref, full.at[:, span(dt, 0), :], tt_ss.at[j, dt, 0], tt_rs.at[j, dt, 0],
                tp_dev(-dt),
            ))
    for ref, full in tokens:
        full[:, 0:tok, :] = ref[...]

    row_tile = tile_of(rows, 256)

    def gather_dot(g, block, q, first=False):
        b = member(q)
        out, full = ((pre, xg), (agr, cg))[g]

        @pl.loop(0, rows // row_tile)
        def _(i):
            part = pl.ds(pl.multiple_of(i * row_tile, row_tile), row_tile)
            lhs = full[b, part, :]
            if g == 0:
                val = jnp.dot(lhs, block[...], preferred_element_type=F32)
            else:
                val = lax.dot_general(lhs, block[...], NT, preferred_element_type=F32)
            if first:
                out[part, :] = val
            else:
                out[part, :] += val

    def finish_tokens():
        for dr in range(1, R):
            for j, (ref, full) in enumerate(tokens):
                rep_copies[j, dr].wait_recv()
                for dt in range(1, T):
                    tp_copies[j, dt, dr] = go(remote(
                        full.at[:, span(0, dr), :], full.at[:, span(dt, dr), :],
                        tt_ss.at[j, dt, dr], tt_rs.at[j, dt, dr], tp_dev(-dt),
                    ))
        for copy in tp_copies.values():
            copy.wait_recv()

        @pl.loop(0, n)
        def _(b):
            xt[b] = xg[b].T

        gather_dot(0, u_ref, 0, True)
        gather_dot(1, d_ref, 0, True)

    for s in range(1, hops + 1):
        for i, (g, sign, k) in enumerate(streams):
            if s <= k:
                flying[i, s].wait_recv()
                if s < k:
                    flying[i, s + 1] = go(gather_copy(i, s + 1))
        if s == 1:
            finish_tokens()
        for i, (g, sign, k) in enumerate(streams):
            if s <= k:
                gather_dot(g, held[g].at[slot(sign, s)], -sign * s)

    act_tile = tile_of(rows, 128)

    @pl.loop(0, rows // act_tile)
    def _(i):
        part = pl.ds(pl.multiple_of(i * act_tile, act_tile), act_tile)
        active = jnp.maximum(pre[part, :], 0.0)
        pg[part, :] = (2.0 * active * agr[part, :]).astype(BF16)
        at[:, part] = (active * active).astype(BF16).T

    def grad_block(g, q, dst, arrived):
        b = member(q)
        height = (db, hb)[g]
        tile = tile_of(height, 256)

        @pl.loop(0, height // tile)
        def _(i):
            part = pl.ds(pl.multiple_of(i * tile, tile), tile)
            if g == 0:
                val = jnp.dot(xt[b, part, :], pg[...], preferred_element_type=F32)
            else:
                val = jnp.dot(at[part, :], cg[b], preferred_element_type=F32)
            for a in arrived:
                val = val + a[part, :].astype(F32)
            dst[part, :] = val.astype(BF16)

    rs_send, rs_recv = (us, ds_), (ur, dr_)

    def rs_index(i, s):
        g, sign, _ = streams[i]
        return s - 1 if sign > 0 else (long, short)[g] + s - 1

    reducing = {}

    def reduce_step(i, s):
        g, sign, k = streams[i]
        arrived = []
        if s > 1:
            reducing[i, s - 1].wait_recv()
            arrived = [rs_recv[g].at[rs_index(i, s - 1)]]
        mine = rs_send[g].at[rs_index(i, s)]
        grad_block(g, sign * (k - s + 1), mine, arrived)
        reducing[i, s] = go(remote(
            mine, rs_recv[g].at[rs_index(i, s)], rs_ss.at[i, s - 1], rs_rs.at[i, s - 1],
            ring_dev(sign),
        ))

    for i, (g, sign, k) in enumerate(streams):
        if k >= 1:
            reduce_step(i, 1)

    for q in range(n):
        block = u_ref if q == 0 else ug.at[q - 1]
        b = member(q)

        @pl.loop(0, rows // row_tile)
        def _(i):
            part = pl.ds(pl.multiple_of(i * row_tile, row_tile), row_tile)
            igp[b, part, :] = lax.dot_general(
                pg[part, :], block[...], NT, preferred_element_type=F32
            ).astype(BF16)

    wide = R * tok
    it_copies = [
        go(remote(
            igp.at[:, pl.ds(dt * wide, wide), :], itr.at[dt - 1],
            it_ss.at[dt], it_rs.at[dt], tp_dev(dt),
        ))
        for dt in range(1, T)
    ]
    ir_copies = []

    def finish_tp():
        for copy in it_copies:
            copy.wait_recv()

        @pl.loop(0, n)
        def _(b):
            for dr in range(R):
                part = pl.ds(dr * tok, tok)
                val = igp[b, part, :].astype(F32)
                for dt in range(1, T):
                    val = val + itr[dt - 1, b, part, :].astype(F32)
                isum[dr, b] = val.astype(BF16)

        for dr in range(1, R):
            ir_copies.append(go(remote(
                isum.at[dr], irr.at[dr - 1], ir_ss.at[dr], ir_rs.at[dr], rep_dev(dr)
            )))

    def finish_rep():
        for copy in ir_copies:
            copy.wait_recv()

        @pl.loop(0, n)
        def _(b):
            val = isum[0, b].astype(F32)
            for dr in range(1, R):
                val = val + irr[dr - 1, b].astype(F32)
            ig_ref[b] = val.astype(BF16)

    finish_tp()
    for s in range(2, hops + 1):
        for i, (g, sign, k) in enumerate(streams):
            if s <= k:
                reduce_step(i, s)
        if s == 2:
            finish_rep()
    if hops < 2:
        finish_rep()

    finals = ((fu, fur, gu_ref), (fd, fdr, gd_ref))
    fin_copies = {}
    for g, (mine, theirs, out) in enumerate(finals):
        arrived = []
        for i, (h, sign, k) in enumerate(streams):
            if h == g and k >= 1:
                reducing[i, k].wait_recv()
                arrived.append(rs_recv[g].at[rs_index(i, k)])
        grad_block(g, 0, mine, arrived)
        for dr in range(1, R):
            fin_copies[g, dr] = go(remote(
                mine, theirs.at[dr - 1], f_ss.at[g, dr], f_rs.at[g, dr], rep_dev(-dr)
            ))
    for g, (mine, theirs, out) in enumerate(finals):
        out[r] = mine[...]
    for g, (mine, theirs, out) in enumerate(finals):
        for dr in range(1, R):
            fin_copies[g, dr].wait_recv()
            out[lax.rem(r + dr, R)] = theirs[dr - 1]
    for copy in sends:
        copy.wait_send()


def shards(inputs, cotangent, up_weight, down_weight):
    R, n, T = lax.axis_size("rep"), lax.axis_size("fs"), lax.axis_size("tp")
    tok, D = inputs.shape
    db, hb = up_weight.shape[0], up_weight.shape[1] // R
    rows = R * T * tok
    r = lax.axis_index("rep")
    by_block = lambda a: a.reshape(tok, n, db).swapaxes(0, 1)
    up = lax.dynamic_slice_in_dim(up_weight, r * hb, hb, 1)
    down = lax.dynamic_slice_in_dim(down_weight, r * hb, hb, 0)
    V, S = pltpu.VMEM, pltpu.SemaphoreType.DMA
    hops = max(n // 2, 1)
    m = max(n - 1, 1)
    scratch = [
        V((n, rows, db), BF16), V((n, rows, db), BF16), V((n, db, rows), BF16),
        V((m, db, hb), BF16), V((m, hb, db), BF16),
        V((rows, hb), F32), V((rows, hb), F32), V((rows, hb), BF16), V((hb, rows), BF16),
        V((n, rows, db), BF16), V((max(T - 1, 1), n, R * tok, db), BF16),
        V((R, n, tok, db), BF16), V((max(R - 1, 1), n, tok, db), BF16),
        V((m, db, hb), BF16), V((m, db, hb), BF16), V((m, hb, db), BF16), V((m, hb, db), BF16),
        V((db, hb), BF16), V((hb, db), BF16),
        V((max(R - 1, 1), db, hb), BF16), V((max(R - 1, 1), hb, db), BF16),
        S((4, hops)), S((4, hops)), S((4, hops)), S((4, hops)),
        S((2, R)), S((2, R)), S((2, T, R)), S((2, T, R)),
        S((T,)), S((T,)), S((R,)), S((R,)), S((2, R)), S((2, R)),
    ]
    vmem = pl.BlockSpec(memory_space=pltpu.VMEM)
    ig, gu, gd = pl.pallas_call(
        functools.partial(kernel, R, n, T),
        out_shape=(
            jax.ShapeDtypeStruct((n, tok, db), BF16),
            jax.ShapeDtypeStruct((R, db, hb), BF16),
            jax.ShapeDtypeStruct((R, hb, db), BF16),
        ),
        in_specs=[vmem] * 4,
        out_specs=(vmem,) * 3,
        scratch_shapes=scratch,
        compiler_params=pltpu.CompilerParams(
            collective_id=0, has_side_effects=True, vmem_limit_bytes=60 * 2**20
        ),
    )(by_block(inputs), by_block(cotangent), up, down)
    total_tokens = tok * R * n * T
    loss_scale = 1.0 / math.sqrt(total_tokens)
    input_grad = ig.swapaxes(0, 1).reshape(tok, D)
    up_grad = gu.swapaxes(0, 1).reshape(db, R * hb).astype(F32) * loss_scale
    down_grad = gd.reshape(R * hb, db).astype(F32) * loss_scale
    return input_grad, up_grad, down_grad


def solution(mesh):
    token, up, down = P(("rep", "fs", "tp"), None), P("fs", "tp"), P("tp", "fs")
    return jax.shard_map(
        shards,
        mesh=mesh,
        in_specs=(token, token, up, down),
        out_specs=(token, up, down),
        check_vma=False,
    )
```

time: 979 us -> 210 us (0.21)
  waiting for transfers between devices: 919 us -> 0 us
  Pallas kernels: 0 us -> 193 us
  matrix products: 36.3 us -> 0 us
  between operations: 14.2 us -> 0.7 us
    reduce_scatter x3 -> x0, waiting for transfers between devices: 555 us -> none  [the longest x1 283 us: shards(): lax.psum_scatter(lax.dot_general(columns, pre_grad, (((0,), (0,)), ((), (...]
    all_gather x4 -> x0, waiting for transfers between devices: 260 us -> none  [the longest x1 128 us: shards(): up_whole = lax.all_gather(up_weight, 'fs', axis=0, tiled=True)]
    pallas_call x0 -> x1, Pallas kernels: none -> 193 us  [shards(): pl.pallas_call(functools.partial(kernel, R, n, T), out_shape=(jax.ShapeDt...]
    psum x1 -> x0, waiting for transfers between devices: 102 us -> none  [shards(): up_grad, down_grad = lax.psum((up_piece, down_piece), 'rep')]
    dot_general x5 -> x0, matrix products: 36.3 us -> none  [the longest x1 9.36 us: shards(): lax.dot_general(activation, grad_rows, (((0,), (0,)), ((), ())), preferre...]
  transfers between devices with their start and end apart: 8 -> 0, of which waited for: 8 -> 0; matrix products, arithmetic and copies ran while one was open for 4% -> 0% of each run, Pallas kernels for 0% -> 0%
where the time goes in v1:
time: 210 us; the launch traced here: 209 us
  Pallas kernels  193 us (92%)
  local copies, waits for them, and re-layouts  12.5 us (6%)
  other arithmetic  2.97 us (1%)
    pallas_call x1, Pallas kernels, shards(): pl.pallas_call(functools.partial(kernel, R, n, T), out_shape=(jax.ShapeDt...  193 us
    unnamed x12, local copies, waits for them, and re-layouts  5.7 us

profile of v1, /device:TPU:0, one launch (start us, length us, event | category | flops | bytes accessed | tf_op | source)
XLA Modules:
  0.0 209.5 jit_solution(4535614561273625707)
XLA Ops:
  0.6 0.0 copy-start
  0.6 0.0 copy-start.2
  0.7 1.4 copy.7
  2.1 0.0 copy-start.3
  2.1 1.0 copy.8
  3.1 0.0 copy-done.2
  3.1 0.3 copy.9
  3.4 1.0 copy.10
  4.4 0.0 copy-done
  4.4 0.8 constant_dynamic-slice_fusion.1.u_ref
  5.2 0.0 copy-done.3
  5.2 0.8 constant_dynamic-slice_fusion.d_ref
  6.1 193.3 %shard_map.67 = (bf16[8,128,256]{2,1,0:T(8,128)(2,1)}, bf16[2,256,1024]{2,1,0:T(8,128)(2,1)}, bf16[2,1024,256]{2,1,0:T(8,128)(2,1)}) custom-call(bf16[8,128,256]{2,1,0:T(8,128)(2,1)} %bitcast.15, bf16[8,128,256]{2,1,0:T(8,128)(2,1)} %bitcast.16, bf16[256,1024]{1,0:T(8,128)(2,1)} %constant_dynamic-slice_fusion.1.u_ref, ...), custom_call_target="tpu_custom_call" | custom-call | tf_op jit(solution)/shard_map/pallas_call | solution.py:332
  199.4 1.3 copy.11
  200.7 1.0 copy.13
  201.7 1.5 multiply_bitcast_fusion
  203.2 1.8 copy.12
  205.0 0.0 copy-start.1
  205.0 3.0 %copy.14 = f32[256,2048]{1,0:T(8,128)} copy(f32[256,2048]{0,1:T(8,128)} %bitcast.10) | data formatting | bytes 4194304
  208.0 0.0 copy-done.1
  208.0 1.5 convert_multiply_fusion
Async XLA Ops:
  0.6 3.8 %copy-start = (bf16[256,2048]{1,0:T(8,128)(2,1)S(1)}, bf16[256,2048]{1,0:T(8,128)(2,1)}, u32[]{:S(2)}) copy-start(bf16[256,2048]{1,0:T(8,128)(2,1)} %param.6) | copy-start | bytes 3145732
  0.6 2.5 %copy-start.2 = (bf16[128,2048]{1,0:T(8,128)(2,1)S(1)}, bf16[128,2048]{1,0:T(8,128)(2,1)}, u32[]{:S(2)}) copy-start(bf16[128,2048]{1,0:T(8,128)(2,1)} %param.5) | copy-start | bytes 1572868
  2.1 3.2 %copy-start.3 = (bf16[2048,256]{1,0:T(8,128)(2,1)S(1)}, bf16[2048,256]{1,0:T(8,128)(2,1)}, u32[]{:S(2)}) copy-start(bf16[2048,256]{1,0:T(8,128)(2,1)} %param.7) | copy-start | bytes 3145732
  205.0 3.0 %copy-start.1 = (bf16[2,1024,256]{2,1,0:T(8,128)(2,1)S(1)}, bf16[2,1024,256]{2,1,0:T(8,128)(2,1)}, u32[]{:S(2)}) copy-start(bf16[2,1024,256]{2,1,0:T(8,128)(2,1)} %get-tuple-element.8) | copy-start | bytes 3145732

commit v2 on v1

v2 whole, which is shorter than its diff:
```python
import functools
import math

import jax
import jax.numpy as jnp
from jax import lax
from jax.experimental import pallas as pl
from jax.experimental.pallas import tpu as pltpu
from jax.sharding import PartitionSpec as P

MESH = pl.DeviceIdType.MESH
CHUNKS = 2
BF16, F32 = jnp.bfloat16, jnp.float32
NT = (((1,), (1,)), ((), ()))


def ring_place(f, n):
    odd = lax.rem(f, 2)
    half = lax.div(f, 2)
    return half * (1 - odd) + (n - 1 - half) * odd


def ring_member(p, n):
    back = lax.div(p, (n + 1) // 2)
    return 2 * p * (1 - back) + (2 * n - 1 - 2 * p) * back


def tile_of(size, most):
    while size % most:
        most //= 2
    return most


def kernel(
    R, n, T,
    x_ref, c_ref, u_ref, d_ref,
    ig_ref, gu_ref, gd_ref,
    xg, cg, xt, ug, dg, pre, agr, pg, at,
    igp, itr, isum, irr, us, ur, ds_, dr_, fu, fd, fur, fdr,
    ag_ss, ag_rs, rs_ss, rs_rs, tr_ss, tr_rs, tt_ss, tt_rs,
    it_ss, it_rs, ir_ss, ir_rs, f_ss, f_rs,
):
    r, f, t = lax.axis_index("rep"), lax.axis_index("fs"), lax.axis_index("tp")
    tok, db = x_ref.shape[0], u_ref.shape[0]
    C, w = pre.shape[0], pre.shape[2]
    hb = C * w
    rows = R * T * tok

    def hidden(place, ch):
        return pl.ds(pl.multiple_of(place * hb + ch * w, w), w)

    for ref, full in ((x_ref, xg), (c_ref, cg)):
        for q in range(n):
            full[q, 0:tok, :] = ref[:, q * db:(q + 1) * db]
    p = ring_place(f, n)

    def member(q):
        return ring_member(lax.rem(p + q + n, n), n)

    def ring_dev(sign):
        return (r, member(sign), t)

    def rep_dev(q):
        return (lax.rem(r + q + R, R), f, t)

    def tp_dev(q):
        return (r, f, lax.rem(t + q + T, T))

    barrier = pltpu.get_barrier_semaphore()
    peers = [ring_dev(1), ring_dev(-1)]
    peers += [rep_dev(q) for q in range(1, R)] + [tp_dev(q) for q in range(1, T)]
    for peer in peers:
        pl.semaphore_signal(barrier, inc=1, device_id=peer, device_id_type=MESH)
    pl.semaphore_wait(barrier, len(peers))

    def remote(src, dst, ssem, rsem, dev):
        return pltpu.make_async_remote_copy(
            src_ref=src, dst_ref=dst, send_sem=ssem, recv_sem=rsem,
            device_id=dev, device_id_type=MESH,
        )

    long, short = n // 2, (n - 1) // 2
    streams = [(0, 1, long), (0, -1, short), (1, 1, short), (1, -1, long)]
    hops = max(long, short)
    def own(g, ch):
        return u_ref.at[:, hidden(r, ch)] if g == 0 else d_ref.at[hidden(r, ch), :]

    held = (ug, dg)

    def slot(sign, s):
        return (n - s if sign > 0 else s) - 1

    def gather_copy(ch, i, s):
        g, sign, _ = streams[i]
        src = own(g, ch) if s == 1 else held[g].at[slot(sign, s - 1), ch]
        return remote(
            src, held[g].at[slot(sign, s), ch],
            ag_ss.at[ch, i, s - 1], ag_rs.at[ch, i, s - 1], ring_dev(sign),
        )

    sends = []

    def go(copy):
        copy.start()
        sends.append(copy)
        return copy

    flying = {}

    def gather_first(ch):
        for i, (g, sign, k) in enumerate(streams):
            if k >= 1:
                flying[ch, i, 1] = go(gather_copy(ch, i, 1))

    gather_first(0)

    tokens = tuple((full.at[:, 0:tok, :], full) for full in (xg, cg))

    def span(dt, dr):
        return pl.ds((dt * R + dr) * tok, tok)

    rep_copies = {}
    for dr in range(1, R):
        for j, (ref, full) in enumerate(tokens):
            rep_copies[j, dr] = go(remote(
                ref, full.at[:, span(0, dr), :], tr_ss.at[j, dr], tr_rs.at[j, dr], rep_dev(-dr)
            ))
    tp_copies = {}
    for dt in range(1, T):
        for j, (ref, full) in enumerate(tokens):
            tp_copies[j, dt, 0] = go(remote(
                ref, full.at[:, span(dt, 0), :], tt_ss.at[j, dt, 0], tt_rs.at[j, dt, 0],
                tp_dev(-dt),
            ))

    row_tile = tile_of(rows, 256)

    def gather_dot(ch, g, block, q, first=False):
        b = member(q)
        out, full = ((pre, xg), (agr, cg))[g]

        @pl.loop(0, rows // row_tile)
        def _(i):
            part = pl.ds(pl.multiple_of(i * row_tile, row_tile), row_tile)
            lhs = full[b, part, :]
            if g == 0:
                val = jnp.dot(lhs, block[...], preferred_element_type=F32)
            else:
                val = lax.dot_general(lhs, block[...], NT, preferred_element_type=F32)
            if first:
                out[ch, part, :] = val
            else:
                out[ch, part, :] += val

    def finish_tokens():
        for dr in range(1, R):
            for j, (ref, full) in enumerate(tokens):
                rep_copies[j, dr].wait_recv()
                for dt in range(1, T):
                    tp_copies[j, dt, dr] = go(remote(
                        full.at[:, span(0, dr), :], full.at[:, span(dt, dr), :],
                        tt_ss.at[j, dt, dr], tt_rs.at[j, dt, dr], tp_dev(-dt),
                    ))
        for copy in tp_copies.values():
            copy.wait_recv()

        @pl.loop(0, n)
        def _(b):
            xt[b] = xg[b].T

        for ch in range(C):
            gather_dot(ch, 0, own(0, ch), 0, True)
            gather_dot(ch, 1, own(1, ch), 0, True)

    act_tile = tile_of(rows, 128)

    def activate(ch):
        @pl.loop(0, rows // act_tile)
        def _(i):
            part = pl.ds(pl.multiple_of(i * act_tile, act_tile), act_tile)
            active = jnp.maximum(pre[ch, part, :], 0.0)
            pg[ch, part, :] = (2.0 * active * agr[ch, part, :]).astype(BF16)
            at[ch, :, part] = (active * active).astype(BF16).T

    def gather(ch, before_last):
        for s in range(1, hops + 1):
            if s == hops:
                before_last()
            for i, (g, sign, k) in enumerate(streams):
                if s <= k:
                    flying[ch, i, s].wait_recv()
                    if s < k:
                        flying[ch, i, s + 1] = go(gather_copy(ch, i, s + 1))
            if s == 1 and ch == 0:
                finish_tokens()
            for i, (g, sign, k) in enumerate(streams):
                if s <= k:
                    gather_dot(ch, g, held[g].at[slot(sign, s), ch], -sign * s)
        if hops == 0:
            if ch == 0:
                finish_tokens()
            before_last()
        activate(ch)

    def grad_block(ch, g, q, dst, arrived):
        b = member(q)
        height = (db, w)[g]
        tile = tile_of(height, 256)

        @pl.loop(0, height // tile)
        def _(i):
            part = pl.ds(pl.multiple_of(i * tile, tile), tile)
            if g == 0:
                val = jnp.dot(xt[b, part, :], pg[ch], preferred_element_type=F32)
            else:
                val = jnp.dot(at[ch, part, :], cg[b], preferred_element_type=F32)
            for a in arrived:
                val = val + a[part, :].astype(F32)
            dst[part, :] = val.astype(BF16)

    rs_send, rs_recv = (us, ds_), (ur, dr_)

    def rs_index(i, s):
        g, sign, _ = streams[i]
        return s - 1 if sign > 0 else (long, short)[g] + s - 1

    reducing = {}

    def reduce_step(ch, i, s):
        g, sign, k = streams[i]
        arrived = []
        if s > 1:
            reducing[ch, i, s - 1].wait_recv()
            arrived = [rs_recv[g].at[rs_index(i, s - 1), ch]]
        mine = rs_send[g].at[rs_index(i, s), ch]
        grad_block(ch, g, sign * (k - s + 1), mine, arrived)
        reducing[ch, i, s] = go(remote(
            mine, rs_recv[g].at[rs_index(i, s), ch],
            rs_ss.at[ch, i, s - 1], rs_rs.at[ch, i, s - 1], ring_dev(sign),
        ))

    def reduce_all(ch, s):
        for i, (g, sign, k) in enumerate(streams):
            if s <= k:
                reduce_step(ch, i, s)

    for ch in range(C):
        if ch + 1 < C:
            gather(ch, functools.partial(gather_first, ch + 1))
        elif C > 1:
            gather(ch, functools.partial(reduce_all, 0, 1))
        else:
            gather(ch, lambda: None)
            reduce_all(ch, 1)

    for q in range(n):
        b = member(q)

        @pl.loop(0, rows // row_tile)
        def _(i):
            part = pl.ds(pl.multiple_of(i * row_tile, row_tile), row_tile)
            val = 0.0
            for ch in range(C):
                block = own(0, ch) if q == 0 else ug.at[q - 1, ch]
                val = val + lax.dot_general(
                    pg[ch, part, :], block[...], NT, preferred_element_type=F32
                )
            igp[b, part, :] = val.astype(BF16)

    wide = R * tok
    it_copies = [
        go(remote(
            igp.at[:, pl.ds(dt * wide, wide), :], itr.at[dt - 1],
            it_ss.at[dt], it_rs.at[dt], tp_dev(dt),
        ))
        for dt in range(1, T)
    ]
    ir_copies = []

    def finish_tp():
        for copy in it_copies:
            copy.wait_recv()

        @pl.loop(0, n)
        def _(b):
            for dr in range(R):
                part = pl.ds(dr * tok, tok)
                val = igp[b, part, :].astype(F32)
                for dt in range(1, T):
                    val = val + itr[dt - 1, b, part, :].astype(F32)
                isum[dr, b] = val.astype(BF16)

        for dr in range(1, R):
            ir_copies.append(go(remote(
                isum.at[dr], irr.at[dr - 1], ir_ss.at[dr], ir_rs.at[dr], rep_dev(dr)
            )))

    def finish_rep():
        for copy in ir_copies:
            copy.wait_recv()

        for b in range(n):
            val = isum[0, b].astype(F32)
            for dr in range(1, R):
                val = val + irr[dr - 1, b].astype(F32)
            ig_ref[:, b * db:(b + 1) * db] = val.astype(BF16)

    finish_tp()

    finals = ((fu, fur, gu_ref), (fd, fdr, gd_ref))
    fin_copies = {}

    def put(g, place, ch, val):
        if g == 0:
            gu_ref[:, hidden(place, ch)] = val
        else:
            gd_ref[hidden(place, ch), :] = val

    def finish(ch, g):
        mine, theirs, out = finals[g]
        arrived = []
        for i, (h, sign, k) in enumerate(streams):
            if h == g and k >= 1:
                reducing[ch, i, k].wait_recv()
                arrived.append(rs_recv[g].at[rs_index(i, k), ch])
        grad_block(ch, g, 0, mine.at[ch], arrived)
        for dr in range(1, R):
            fin_copies[ch, g, dr] = go(remote(
                mine.at[ch], theirs.at[dr - 1, ch],
                f_ss.at[ch, g, dr], f_rs.at[ch, g, dr], rep_dev(-dr),
            ))
        put(g, r, ch, mine[ch])

    for ch in range(C):
        for s in range(2, hops + 1):
            reduce_all(ch, s)
            if ch == 0 and s == 2:
                finish_rep()
        if ch == 0 and hops < 2:
            finish_rep()
        if ch + 1 < C:
            reduce_all(ch + 1, 1)
        for g in range(2):
            finish(ch, g)
    for (ch, g, dr), copy in fin_copies.items():
        _, theirs, out = finals[g]
        copy.wait_recv()
        put(g, lax.rem(r + dr, R), ch, theirs[dr - 1, ch])
    for copy in sends:
        copy.wait_send()


def shards(inputs, cotangent, up_weight, down_weight):
    R, n, T = lax.axis_size("rep"), lax.axis_size("fs"), lax.axis_size("tp")
    tok, D = inputs.shape
    db, hb = up_weight.shape[0], up_weight.shape[1] // R
    rows = R * T * tok
    C = tile_of(hb // 128, CHUNKS) if hb > 128 else 1
    w = hb // C
    V, S = pltpu.VMEM, pltpu.SemaphoreType.DMA
    hops = max(n // 2, 1)
    m = max(n - 1, 1)
    scratch = [
        V((n, rows, db), BF16), V((n, rows, db), BF16), V((n, db, rows), BF16),
        V((m, C, db, w), BF16), V((m, C, w, db), BF16),
        V((C, rows, w), F32), V((C, rows, w), F32), V((C, rows, w), BF16), V((C, w, rows), BF16),
        V((n, rows, db), BF16), V((max(T - 1, 1), n, R * tok, db), BF16),
        V((R, n, tok, db), BF16), V((max(R - 1, 1), n, tok, db), BF16),
        V((m, C, db, w), BF16), V((m, C, db, w), BF16),
        V((m, C, w, db), BF16), V((m, C, w, db), BF16),
        V((C, db, w), BF16), V((C, w, db), BF16),
        V((max(R - 1, 1), C, db, w), BF16), V((max(R - 1, 1), C, w, db), BF16),
        S((C, 4, hops)), S((C, 4, hops)), S((C, 4, hops)), S((C, 4, hops)),
        S((2, R)), S((2, R)), S((2, T, R)), S((2, T, R)),
        S((T,)), S((T,)), S((R,)), S((R,)), S((C, 2, R)), S((C, 2, R)),
    ]
    vmem = pl.BlockSpec(memory_space=pltpu.VMEM)
    ig, gu, gd = pl.pallas_call(
        functools.partial(kernel, R, n, T),
        out_shape=(
            jax.ShapeDtypeStruct((tok, D), BF16),
            jax.ShapeDtypeStruct((db, R * hb), BF16),
            jax.ShapeDtypeStruct((R * hb, db), BF16),
        ),
        in_specs=[vmem] * 4,
        out_specs=(vmem,) * 3,
        scratch_shapes=scratch,
        compiler_params=pltpu.CompilerParams(
            collective_id=0, has_side_effects=True, vmem_limit_bytes=60 * 2**20
        ),
    )(inputs, cotangent, up_weight, down_weight)
    total_tokens = tok * R * n * T
    loss_scale = 1.0 / math.sqrt(total_tokens)
    return ig, gu.astype(F32) * loss_scale, gd.astype(F32) * loss_scale


def solution(mesh):
    token, up, down = P(("rep", "fs", "tp"), None), P("fs", "tp"), P("tp", "fs")
    return jax.shard_map(
        shards,
        mesh=mesh,
        in_specs=(token, token, up, down),
        out_specs=(token, up, down),
        check_vma=False,
    )
```

time: 210 us -> 202 us (0.962)
  local copies, waits for them, and re-layouts: 12.5 us -> 0.8 us
  Pallas kernels: 193 us -> 196 us
    unnamed x12 -> x5, local copies, waits for them, and re-layouts: 5.7 us -> 0.8 us
    pallas_call x1, Pallas kernels: 193 us -> 196 us  [shards(): pl.pallas_call(functools.partial(kernel, R, n, T), out_shape=(jax.ShapeDt...]
where the time goes in v2:
time: 202 us
  Pallas kernels  196 us (97%)
  other arithmetic  4.33 us (2%)
    pallas_call x1, Pallas kernels, shards(): pl.pallas_call(functools.partial(kernel, R, n, T), out_shape=(jax.ShapeDt...  196 us
    mul x2, other arithmetic, shards(): return (ig, gu.astype(F32) * loss_scale, gd.astype(F32) * loss_scale)  4.33 us

profile of v2, /device:TPU:0, one launch (start us, length us, event | category | flops | bytes accessed | tf_op | source)
XLA Modules:
  0.0 201.8 jit_solution(6366145026224585925)
XLA Ops:
  0.6 196.0 %shard_map.67 = (bf16[128,2048]{1,0:T(8,128)(2,1)}, bf16[256,2048]{1,0:T(8,128)(2,1)}, bf16[2048,256]{1,0:T(8,128)(2,1)}) custom-call(bf16[128,2048]{1,0:T(8,128)(2,1)} %x_ref.1, bf16[128,2048]{1,0:T(8,128)(2,1)} %c_ref.1, bf16[256,2048]{1,0:T(8,128)(2,1)} %u_ref.1, bf16[2048,256]{1,0:T(8,128)(2,1)} %d_ref.1), custom_call_target="tpu_custom_call" | custom-call | tf_op jit(solution)/shard_map/pallas_call | solution.py:378
  196.7 0.0 copy-start
  196.7 2.9 %convert_multiply_fusion.1 = f32[256,2048]{1,0:T(8,128)} fusion(bf16[256,2048]{1,0:T(8,128)(2,1)} %get-tuple-element.7), kind=kLoop, calls=%fused_computation.1 | loop fusion | flops 1048576 | bytes 3145728 | tf_op jit(solution)/shard_map/mul | solution.py:394
  199.6 0.0 copy-done
  199.6 0.0 copy-start.1
  199.6 1.5 convert_multiply_fusion
  201.0 0.0 copy-done.1
  201.0 0.8 copy.8
Async XLA Ops:
  196.7 2.9 %copy-start = (bf16[2048,256]{1,0:T(8,128)(2,1)S(1)}, bf16[2048,256]{1,0:T(8,128)(2,1)}, u32[]{:S(2)}) copy-start(bf16[2048,256]{1,0:T(8,128)(2,1)} %get-tuple-element.8) | copy-start | bytes 3145732
  199.6 1.5 copy-start.1
